TPU v7x, 512 devices: a whole 4x4x16 slice. The times are simulated.
512 devices in a mesh: sp: 64 (over z, y), tp: 8 (over x, core).
Axes of the slice: x: 4, y: 4, z: 16, core: 2. Of those that a mesh axis runs over, the one named last changes fastest.
Arguments:
- stream: bfloat16 [8192, 2048], P('sp'), may hold values from -6 to 6
- query_narrow: bfloat16 [8192, 512], P('sp', 'tp'), may hold values from -7 to 7
- query_broad: bfloat16 [8192, 1024], P('sp', 'tp'), may hold values from -7 to 7
- key_narrow: bfloat16 [8192, 512], P('sp', 'tp'), may hold values from -7 to 7
- key_broad: bfloat16 [8192, 1024], P('sp', 'tp'), may hold values from -7 to 7
- value_narrow: bfloat16 [8192, 512], P('sp', 'tp'), may hold values from -6 to 6
- value_broad: bfloat16 [8192, 1024], P('sp', 'tp'), may hold values from -6 to 6
- key_offsets: float32 [8192, 16], P('sp', 'tp'), may hold values from -20 to 0
- out_narrow: bfloat16 [512, 2048], P('tp'), may hold values from -0.4375 to 0.4375
- out_broad: bfloat16 [1024, 2048], P('tp'), may hold values from -0.4375 to 0.4375
- norm_gain: float32 [2048], replicated, may hold values from 0.1 to 1.9
- gate_weight: bfloat16 [2048, 3072], P('sp', 'tp'), may hold values from -0.125 to 0.125
- up_weight: bfloat16 [2048, 3072], P('sp', 'tp'), may hold values from -0.125 to 0.125
- down_weight: bfloat16 [3072, 2048], P('tp', 'sp'), may hold values from -0.21875 to 0.21875
Outputs:
- result: bfloat16 [8192, 2048], P(('sp', 'tp'))
All inputs are finite; a program needn't handle non-finite values.
Results may differ from a plain program's by a relative error of at most 0.028.
Values may be sent and summed in bfloat16 or wider, within the bound.
A program may use at most 64 MiB of HBM per device.

v0:
```python
import jax
import jax.numpy as jnp
from jax import lax
from jax.sharding import Mesh
from jax.sharding import PartitionSpec as P

NARROW_SIZE = 64
BROAD_SIZE = 128
SP = ("sp_0", "sp_1")
SP_TP = ("sp_0", "sp_1", "tp")
grain = 8
block_keys = 512
norm_eps = 1e-06


def laid_out(blocks, dim):
    blocks = jnp.moveaxis(blocks, 0, dim)
    shape = blocks.shape
    return blocks.reshape(*shape[:dim], shape[dim] * shape[dim + 1], *shape[dim + 2 :])


def gather_in_order(shard, axes, sequence):
    blocks = shard[None]
    for k in sequence:
        blocks = lax.all_gather(blocks, axes[k], axis=0, tiled=True)
    carried = [lax.axis_size(axes[k]) for k in reversed(sequence)]
    blocks = blocks.reshape(*carried, *shard.shape)
    turned = sorted(range(len(sequence)), key=lambda place: sequence[len(sequence) - 1 - place])
    return blocks.transpose(*turned, *range(len(sequence), blocks.ndim)).reshape(-1, *shard.shape)


def whole_of(shard, axes, sequence, dim):
    return laid_out(gather_in_order(shard, axes, sequence), dim)


def sent_to_all(shard, axis):
    peers = lax.axis_size(axis)
    return lax.all_to_all(
        jnp.broadcast_to(shard[None], (peers, *shard.shape)), axis, 0, 0, tiled=True
    )


def over_copies(shard, axis):
    return sent_to_all(shard, axis).astype(jnp.float32).sum(axis=0)


def in_one_piece(arrays, axis, dim, along):
    widths = [a.shape[along] for a in arrays]
    both = jnp.concatenate(arrays, axis=along)
    filled = lax.all_gather(both, axis, axis=dim, tiled=True)
    return tuple(jnp.split(filled, [sum(widths[:k]) for k in range(1, len(widths))], axis=along))


def gather_axes(shard, axes, dim):
    filled = shard
    for number in range(len(axes) - 1, -1, -1):
        filled = lax.all_gather(filled, axes[number], axis=dim, tiled=True)
    return filled


def cut_along(shard, dim, peers):
    shape = shard.shape
    blocks = shard.reshape(*shape[:dim], peers, shape[dim] // peers, *shape[dim + 1 :])
    return jnp.moveaxis(blocks, dim, 0)


def summed_on_arrival(shard, axis, dim):
    peers = lax.axis_size(axis)
    blocks = lax.all_to_all(cut_along(shard, dim, peers), axis, 0, 0, tiled=True)
    return jnp.sum(blocks.astype(jnp.float32), axis=0)


def block_plan(length):
    return (length // block_keys, block_keys)


def slice_rows(array, first, count):
    return lax.dynamic_slice_in_dim(array, first, count, 0)


def head_logs(queries, keys_block, offset_block, positions, key_positions, scale):
    logits = (
        jnp.einsum("qhd,khd->hqk", queries, keys_block, preferred_element_type=jnp.float32) * scale
    )
    logits = logits + jnp.transpose(offset_block)[:, None, :]
    causal = (key_positions[None, :] < positions[:, None])[None, :, :]
    lognot = jnp.where(causal, jax.nn.log_sigmoid(-logits), 0.0)
    return (logits, causal, lognot)


def sub_totals(lognot):
    heads, count, length = lognot.shape
    return lognot.reshape(heads, count, length // grain, grain).sum(axis=3)


def weighted_values(logits, causal, lognot, after, values):
    heads, count, length = lognot.shape
    grouped = lognot.reshape(heads, count, length // grain, grain)
    within = lax.cumsum(grouped, axis=3, reverse=True) - grouped
    later = (within + after[:, :, :, None]).reshape(heads, count, length)
    weights = jnp.where(causal, jnp.exp(jax.nn.log_sigmoid(logits) + later), 0.0).astype(
        jnp.bfloat16
    )
    return jnp.einsum("hqk,khd->qhd", weights, values, preferred_element_type=jnp.float32)


def local(
    stream,
    query_narrow,
    query_broad,
    key_narrow,
    key_broad,
    value_narrow,
    value_broad,
    key_offsets,
    out_narrow,
    out_broad,
    norm_gain,
    gate_weight,
    up_weight,
    down_weight,
):
    rows = stream.shape[0]
    heads = query_narrow.shape[1] // NARROW_SIZE
    shaped_narrow = query_narrow.reshape(rows, heads, NARROW_SIZE)
    shaped_broad = query_broad.reshape(rows, heads, BROAD_SIZE)
    positions = lax.axis_index(SP) * rows + jnp.arange(rows, dtype=jnp.int32)
    scale_narrow = NARROW_SIZE ** (-0.5)
    scale_broad = BROAD_SIZE ** (-0.5)

    def key_block(keys_narrow, keys_broad, offsets, first, count):
        block_narrow = slice_rows(keys_narrow, first, count).reshape(count, heads, NARROW_SIZE)
        block_broad = slice_rows(keys_broad, first, count).reshape(count, heads, BROAD_SIZE)
        pairs = slice_rows(offsets, first, count).reshape(count, heads, 2)
        return (block_narrow, block_broad, pairs[:, :, 0], pairs[:, :, 1])

    def value_block(values_narrow, values_broad, first, count):
        return (
            slice_rows(values_narrow, first, count).reshape(count, heads, NARROW_SIZE),
            slice_rows(values_broad, first, count).reshape(count, heads, BROAD_SIZE),
        )

    empty_narrow = jnp.zeros((rows, heads, NARROW_SIZE), jnp.float32)
    empty_broad = jnp.zeros((rows, heads, BROAD_SIZE), jnp.float32)
    whole = (
        whole_of(key_narrow, SP, (0, 1), 0),
        whole_of(key_broad, SP, (0, 1), 0),
        whole_of(value_narrow, SP, (0, 1), 0),
        whole_of(value_broad, SP, (0, 1), 0),
        whole_of(key_offsets.astype(jnp.bfloat16), SP, (0, 1), 0).astype(key_offsets.dtype),
    )
    keys_narrow, keys_broad, values_narrow, values_broad, offsets = whole
    steps, span = block_plan(keys_narrow.shape[0])
    running = jnp.zeros((heads, rows), jnp.float32)

    def back_step(index, state):
        first = (steps - 1 - index) * span
        block_narrow, block_broad, offset_narrow, offset_broad = key_block(
            keys_narrow, keys_broad, offsets, first, span
        )
        held_narrow, held_broad = value_block(values_narrow, values_broad, first, span)
        key_positions = first + jnp.arange(span, dtype=jnp.int32)
        logits_narrow, causal_narrow, lognot_narrow = head_logs(
            shaped_narrow, block_narrow, offset_narrow, positions, key_positions, scale_narrow
        )
        logits_broad, causal_broad, lognot_broad = head_logs(
            shaped_broad, block_broad, offset_broad, positions, key_positions, scale_broad
        )
        subs_narrow = sub_totals(lognot_narrow)
        subs_broad = sub_totals(lognot_broad)
        later_narrow = (
            lax.cumsum(subs_narrow, axis=2, reverse=True) - subs_narrow + state[2][:, :, None]
        )
        later_broad = (
            lax.cumsum(subs_broad, axis=2, reverse=True) - subs_broad + state[3][:, :, None]
        )
        return (
            state[0]
            + weighted_values(
                logits_narrow, causal_narrow, lognot_narrow, later_narrow, held_narrow
            ),
            state[1]
            + weighted_values(logits_broad, causal_broad, lognot_broad, later_broad, held_broad),
            state[2] + subs_narrow.sum(axis=2),
            state[3] + subs_broad.sum(axis=2),
        )

    final = lax.fori_loop(0, steps, back_step, (empty_narrow, empty_broad, running, running))
    acc_narrow = final[0]
    acc_broad = final[1]
    attended_narrow = acc_narrow.reshape(rows, heads * NARROW_SIZE).astype(jnp.bfloat16)
    attended_broad = acc_broad.reshape(rows, heads * BROAD_SIZE).astype(jnp.bfloat16)
    share = rows // lax.axis_size("tp")
    own = lax.axis_index("tp") * share
    summed = over_copies(
        (
            jnp.dot(
                slice_rows(attended_narrow, 0, rows), out_narrow, preferred_element_type=jnp.float32
            )
            + jnp.dot(
                slice_rows(attended_broad, 0, rows), out_broad, preferred_element_type=jnp.float32
            )
        ).astype(jnp.bfloat16),
        "tp",
    ).astype(jnp.float32)
    mid_all = (stream.astype(jnp.float32) + summed).astype(jnp.bfloat16)
    middle = mid_all.astype(jnp.float32)
    scaled = middle * lax.rsqrt(jnp.mean(middle * middle, axis=1, keepdims=True) + norm_eps)
    normed = (scaled * norm_gain).astype(jnp.bfloat16)
    mid_own = slice_rows(mid_all, own, share)
    part_gate, part_up = in_one_piece((gate_weight, up_weight), SP, 0, 1)
    gate = jnp.dot(normed, part_gate, preferred_element_type=jnp.float32)
    up = jnp.dot(normed, part_up, preferred_element_type=jnp.float32)
    hidden = (jax.nn.silu(gate) * up).astype(jnp.bfloat16)
    down_full = gather_axes(down_weight, SP, 1)
    mixed = summed_on_arrival(
        jnp.dot(
            slice_rows(hidden, jnp.int32(0), share * lax.axis_size("tp")),
            down_full,
            preferred_element_type=jnp.float32,
        ).astype(jnp.bfloat16),
        "tp",
        0,
    )
    return (mid_own.astype(jnp.float32) + mixed).astype(jnp.bfloat16)


def solution(mesh):
    torus = Mesh(mesh.devices.reshape(16, 4, mesh.shape["tp"]), ("sp_0", "sp_1", "tp"))
    in_specs = (
        P(SP, None),
        P(SP, "tp"),
        P(SP, "tp"),
        P(SP, "tp"),
        P(SP, "tp"),
        P(SP, "tp"),
        P(SP, "tp"),
        P(SP, "tp"),
        P("tp", None),
        P("tp", None),
        P(),
        P(SP, "tp"),
        P(SP, "tp"),
        P("tp", SP),
    )
    out_specs = P(SP_TP, None)
    return jax.shard_map(local, mesh=torus, in_specs=in_specs, out_specs=out_specs, check_vma=False)
```

profile of v0, /device:TPU:1, one launch (start us, length us, event | category | flops | bytes accessed | tf_op | source)
XLA Modules:
  0.0 433.5 jit_solution(11852103382589410577)
XLA Ops:
  6.6 30.8 %all-gather = bf16[2048,64]{0,1:T(8,128)(2,1)S(1)} all-gather(bf16[128,64]{0,1:T(8,128)(2,1)} %param.21), channel_id=2, replica_groups=mesh['sp_0'=16,'sp_1'=4,'tp'=8] {'sp_0'}, dimensions={0}, use_global_device_ids=true | all-gather | bytes 278528 | tf_op jit(solution)/shard_map/all_gather | solution.py:25
  38.2 21.0 %all-gather.1 = bf16[2048,64]{0,1:T(8,128)(2,1)S(1)} all-gather(bf16[128,64]{0,1:T(8,128)(2,1)} %param.19), channel_id=3, replica_groups=mesh['sp_0'=16,'sp_1'=4,'tp'=8] {'sp_0'}, dimensions={0}, use_global_device_ids=true | all-gather | bytes 278528 | tf_op jit(solution)/shard_map/all_gather | solution.py:25
  60.1 26.6 %all-gather.3 = bf16[2048,128]{1,0:T(8,128)(2,1)} all-gather(bf16[128,128]{1,0:T(8,128)(2,1)S(1)} %copy-done.4), channel_id=5, replica_groups=mesh['sp_0'=16,'sp_1'=4,'tp'=8] {'sp_0'}, dimensions={0}, use_global_device_ids=true | all-gather | bytes 557056 | tf_op jit(solution)/shard_map/all_gather | solution.py:25
  86.7 25.8 %all-gather.4 = bf16[2048,128]{1,0:T(8,128)(2,1)} all-gather(bf16[128,128]{1,0:T(8,128)(2,1)S(1)} %copy-done.5), channel_id=6, replica_groups=mesh['sp_0'=16,'sp_1'=4,'tp'=8] {'sp_0'}, dimensions={0}, use_global_device_ids=true | all-gather | bytes 557056 | tf_op jit(solution)/shard_map/all_gather | solution.py:25
  113.4 19.6 %all-gather.2 = bf16[2048,2]{0,1:T(2,128)(2,1)S(1)} all-gather(bf16[128,2]{0,1:T(2,128)(2,1)S(1)} %convert_element_type.77), channel_id=4, replica_groups=mesh['sp_0'=16,'sp_1'=4,'tp'=8] {'sp_0'}, dimensions={0}, use_global_device_ids=true | all-gather | bytes 8704 | tf_op jit(solution)/shard_map/all_gather | solution.py:25
  132.9 12.1 %all_gather.44 = bf16[64,128,2]{1,0,2:T(8,128)(2,1)S(1)} all-gather(bf16[16,128,2]{1,0,2:T(8,128)(2,1)S(1)} %bitcast.157), channel_id=1, replica_groups=mesh['sp_0'=16,'sp_1'=4,'tp'=8] {'sp_1'}, dimensions={0}, use_global_device_ids=true | all-gather | bytes 40960 | tf_op jit(solution)/shard_map/all_gather | solution.py:25
  145.1 3.1 copy.44
  148.3 3.1 copy.46
  152.4 3.2 copy.39
  155.6 37.4 %all-gather.18.cloned.1.call-done = bf16[64,128,128]{2,1,0:T(8,128)(2,1)} async-done(((bf16[16,128,128]{2,1,0:T(8,128)(2,1)}), bf16[64,128,128]{2,1,0:T(8,128)(2,1)}) %all-gather.18.cloned.1.call-update) | async-done | bytes 2097168 | tf_op jit(solution)/shard_map/all_gather | solution.py:25
  193.0 3.3 copy.40
  196.3 116.7 %while.20 = (s32[]{:T(128)}, f32[128,1,64]{0,2,1:T(8,128)S(1)}, f32[128,1,128]{0,2,1:T(8,128)S(1)}, f32[1,128]{1,0:T(1,128)S(1)}, f32[1,128]{1,0:T(1,128)S(1)}, ...) while((s32[]{:T(128)}, f32[128,1,64]{0,2,1:T(8,128)S(1)}, ...), condition=%wide.region_9.10_spmd.clone, body=%wide.region_0.9_spmd.clone.sunk | while | flops 57983880 | bytes 5200671 | solution.py:188
  214.6 1.5 fusion.94
  309.4 1.5 fusion.94
  313.7 2.5 broadcast_in_dim.69
  316.2 5.4 %all-to-all-start = ((bf16[8,128,2048]{2,1,0:T(8,128)(2,1)}), bf16[8,128,2048]{2,1,0:T(8,128)(2,1)}, u32[]{:S(2)}, u32[]{:S(2)}) async-start(bf16[8,128,2048]{2,1,0:T(8,128)(2,1)} %broadcast_in_dim.69), calls=%async_computation | async-start | bytes 8388608 | tf_op jit(solution)/shard_map/all_to_all | solution.py:38
  321.6 10.7 %all_gather.50 = bf16[384,128]{0,1:T(8,128)(2,1)} all-gather(bf16[384,32]{0,1:T(8,128)(2,1)S(1)} %copy-done.8), channel_id=1, replica_groups=mesh['sp_0'=16,'sp_1'=4,'tp'=8] {'sp_1'}, dimensions={1}, use_global_device_ids=true | all-gather | bytes 122880 | tf_op jit(solution)/shard_map/all_gather | solution.py:57
  332.3 38.1 %all-to-all-done = bf16[8,128,2048]{2,1,0:T(8,128)(2,1)} async-done(((bf16[8,128,2048]{2,1,0:T(8,128)(2,1)}), bf16[8,128,2048]{2,1,0:T(8,128)(2,1)}, u32[]{:S(2)}, u32[]{:S(2)}) %all-to-all-start) | async-done | bytes 4194336 | tf_op jit(solution)/shard_map/all_to_all | solution.py:38
  370.4 3.0 convert_reduce_fusion
  374.1 1.9 fusion.41
  376.0 23.2 %all-gather.22.cloned.1.call-done = bf16[384,2048]{0,1:T(8,128)(2,1)} async-done(((bf16[384,128]{0,1:T(8,128)(2,1)}), bf16[384,2048]{0,1:T(8,128)(2,1)}) %all-gather.22.cloned.1.call-update) | async-done | bytes 1572880 | tf_op jit(solution)/shard_map/all_gather | solution.py:57
  399.3 3.7 convolution_convert_fusion
  403.0 13.6 %all-to-all-start.1 = ((bf16[8,16,2048]{2,1,0:T(8,128)(2,1)}), bf16[8,16,2048]{2,1,0:T(8,128)(2,1)S(1)}, u32[]{:S(2)}, u32[]{:S(2)}) async-start(bf16[8,16,2048]{2,1,0:T(8,128)(2,1)} %bitcast.22), calls=%async_computation.1 | async-start | bytes 1048576 | tf_op jit(solution)/shard_map/all_to_all | solution.py:69
  416.6 9.3 %all-to-all-done.1 = bf16[8,16,2048]{2,1,0:T(8,128)(2,1)S(1)} async-done(((bf16[8,16,2048]{2,1,0:T(8,128)(2,1)}), bf16[8,16,2048]{2,1,0:T(8,128)(2,1)S(1)}, u32[]{:S(2)}, u32[]{:S(2)}) %all-to-all-start.1) | async-done | bytes 524320 | tf_op jit(solution)/shard_map/all_to_all | solution.py:69
  (312 shorter events, 117.8 us)
Async XLA Ops:
  6.5 306.8 %copy-start = (bf16[128,2048]{1,0:T(8,128)(2,1)S(1)}, bf16[128,2048]{1,0:T(8,128)(2,1)}, u32[]{:S(2)}) copy-start(bf16[128,2048]{1,0:T(8,128)(2,1)} %param.25) | copy-start | bytes 1572868
  6.5 53.5 %copy-start.4 = (bf16[128,128]{1,0:T(8,128)(2,1)S(1)}, bf16[128,128]{1,0:T(8,128)(2,1)}, u32[]{:S(2)}) copy-start(bf16[128,128]{1,0:T(8,128)(2,1)} %param.22) | copy-start | bytes 98308
  6.5 80.2 %copy-start.5 = (bf16[128,128]{1,0:T(8,128)(2,1)S(1)}, bf16[128,128]{1,0:T(8,128)(2,1)}, u32[]{:S(2)}) copy-start(bf16[128,128]{1,0:T(8,128)(2,1)} %param.20) | copy-start | bytes 98308
  6.5 106.1 %copy-start.7 = (bf16[32,384]{1,0:T(8,128)(2,1)S(1)}, bf16[32,384]{1,0:T(8,128)(2,1)}, u32[]{:S(2)}) copy-start(bf16[32,384]{1,0:T(8,128)(2,1)} %param.27) | copy-start | bytes 73732
  6.5 106.1 %copy-start.6 = (bf16[32,384]{1,0:T(8,128)(2,1)S(1)}, bf16[32,384]{1,0:T(8,128)(2,1)}, u32[]{:S(2)}) copy-start(bf16[32,384]{1,0:T(8,128)(2,1)} %param.28) | copy-start | bytes 73732
  6.5 138.6 %all-gather.12.cloned.1.call-start = ((), (), s32[]{:S(2)}) async-start(), calls=%async_computation.2 | async-start | bytes 1310720 | tf_op jit(solution)/shard_map/all_gather | solution.py:25
  37.4 75.9 %copy-start.11 = (f32[128,2]{0,1:T(2,128)S(1)}, f32[128,2]{0,1:T(2,128)}, u32[]{:S(2)}) copy-start(f32[128,2]{0,1:T(2,128)} %param.23) | copy-start | bytes 3076
  38.2 110.1 %all-gather.14.cloned.1.call-start = ((), (), s32[]{:S(2)}) async-start(), calls=%async_computation.3 | async-start | bytes 1310720 | tf_op jit(solution)/shard_map/all_gather | solution.py:25
  60.0 92.4 %all-gather.16.cloned.1.call-start = ((), (), s32[]{:S(2)}) async-start(), calls=%async_computation.4 | async-start | bytes 2621440 | tf_op jit(solution)/shard_map/all_gather | solution.py:25
  86.6 106.3 %all-gather.18.cloned.1.call-start = ((), (), s32[]{:S(2)}) async-start(), calls=%async_computation.5 | async-start | bytes 2621440 | tf_op jit(solution)/shard_map/all_gather | solution.py:25
  112.6 261.2 %all-gather.20.cloned.1.call-start = ((), (), s32[]{:S(2)}) async-start(), calls=%async_computation.6 | async-start | bytes 3194880 | tf_op jit(solution)/shard_map/all_gather | solution.py:50
  193.0 3.3 copy-start.2
  193.0 3.3 copy-start.9
  196.3 116.7 %copy-start.3 = (bf16[64,2048]{1,0:T(8,128)(2,1)S(1)}, bf16[64,2048]{1,0:T(8,128)(2,1)}, u32[]{:S(2)}) copy-start(bf16[64,2048]{1,0:T(8,128)(2,1)} %param.24) | copy-start | bytes 786436
  316.2 5.4 %copy-start.8 = (bf16[384,32]{0,1:T(8,128)(2,1)S(1)}, bf16[384,32]{0,1:T(8,128)(2,1)}, u32[]{:S(2)}) copy-start(bf16[384,32]{0,1:T(8,128)(2,1)} %param.29) | copy-start | bytes 73732
  316.2 54.2 %all-to-all-start = ((bf16[8,128,2048]{2,1,0:T(8,128)(2,1)}), bf16[8,128,2048]{2,1,0:T(8,128)(2,1)}, u32[]{:S(2)}, u32[]{:S(2)}) async-start(bf16[8,128,2048]{2,1,0:T(8,128)(2,1)} %broadcast_in_dim.69), calls=%async_computation | async-start | bytes 8388608 | tf_op jit(solution)/shard_map/all_to_all | solution.py:38
  321.6 77.7 %all-gather.22.cloned.1.call-start = ((), (), s32[]{:S(2)}) async-start(), calls=%async_computation.7 | async-start | bytes 1671168 | tf_op jit(solution)/shard_map/all_gather | solution.py:57
  332.3 41.1 %copy-start.1 = (bf16[128,2048]{1,0:T(8,128)(2,1)S(1)}, bf16[128,2048]{1,0:T(8,128)(2,1)}, u32[]{:S(2)}) copy-start(bf16[128,2048]{1,0:T(8,128)(2,1)} %param.16) | copy-start | bytes 1572868
  373.4 0.7 copy-start.10
  403.0 23.0 %all-to-all-start.1 = ((bf16[8,16,2048]{2,1,0:T(8,128)(2,1)}), bf16[8,16,2048]{2,1,0:T(8,128)(2,1)S(1)}, u32[]{:S(2)}, u32[]{:S(2)}) async-start(bf16[8,16,2048]{2,1,0:T(8,128)(2,1)} %bitcast.22), calls=%async_computation.1 | async-start | bytes 1048576 | tf_op jit(solution)/shard_map/all_to_all | solution.py:69
Sparse Core Ops, SparseCore 0:
  38.3 34.8 all-gather.11
  75.3 33.8 all-gather.13
  111.3 41.0 all-gather.15
  154.4 38.5 all-gather.17
  195.8 134.4 all-gather.19
  332.4 66.7 all-gather.21
where the time goes:
time: 435 us; the launch traced here: 434 us
  blocking collectives  146 us (34%)
  waiting for transfers between devices  109 us (25%)
  matrix products  93 us (21%)
  other arithmetic  32.7 us (8%)
  starting transfers between devices  19.2 us (4%)
  local copies, waits for them, and re-layouts  17.6 us (4%)
  between operations  13.7 us (3%)
    all_gather x6, blocking collectives, gather_in_order(): blocks = lax.all_gather(blocks, axes[k], axis=0, tiled=True)  136 us
    dot_general x32, matrix products, weighted_values(): jnp.einsum('hqk,khd->qhd', weights, values, preferred_element_type=jnp.fl...  46.6 us
    dot_general x32, matrix products, head_logs(): jnp.einsum('qhd,khd->hqk', queries, keys_block, preferred_element_type=jn...  40.1 us
    all_gather x4, waiting for transfers between devices, gather_in_order(): blocks = lax.all_gather(blocks, axes[k], axis=0, tiled=True)  38.4 us
    all_to_all x1, waiting for transfers between devices, sent_to_all(): lax.all_to_all(jnp.broadcast_to(shard[None], (peers, *shard.shape)), axis...  38.1 us
    all_gather x1, waiting for transfers between devices, gather_axes(): filled = lax.all_gather(filled, axes[number], axis=dim, tiled=True)  23.2 us
    all_to_all x1, starting transfers between devices, summed_on_arrival(): lax.all_to_all(cut_along(shard, dim, peers), axis, 0, 0, tiled=True)  13.6 us
    another operation x32, other arithmetic, weighted_values(): within = lax.cumsum(grouped, axis=3, reverse=True) - grouped  12.2 us
  transfers between devices with their start and end apart: 8, of which 5 were waited for; matrix products, arithmetic and copies ran while one was open for 32% of the time, Pallas kernels for 0%

commit v1 on v0

--- a/solution.py
+++ b/solution.py
@@ -22,7 +22,11 @@
 def gather_in_order(shard, axes, sequence):
     blocks = shard[None]
     for k in sequence:
-        blocks = lax.all_gather(blocks, axes[k], axis=0, tiled=True)
+        x_part = axes[k]
+        now = lax.axis_size(x_part)
+        item_now = jnp.stack([blocks] * now)
+        field_out = lax.all_to_all(item_now, x_part, 0, 0)
+        blocks = jnp.concatenate(field_out, axis=0)
     carried = [lax.axis_size(axes[k]) for k in reversed(sequence)]
     blocks = blocks.reshape(*carried, *shard.shape)
     turned = sorted(range(len(sequence)), key=lambda place: sequence[len(sequence) - 1 - place])

time: 435 us -> 481 us (1.11)
  blocking collectives: 146 us -> 205 us
  waiting for transfers between devices: 109 us -> 83.4 us
  starting transfers between devices: 19.2 us -> 31 us
    all_to_all x0 -> x9, blocking collectives: none -> 194 us  [gather_in_order(): field_out = lax.all_to_all(item_now, x_part, 0, 0)]
    all_gather x6 -> x0, blocking collectives: 136 us -> none  [gather_in_order(): blocks = lax.all_gather(blocks, axes[k], axis=0, tiled=True)]
    all_gather x4 -> x0, waiting for transfers between devices: 38.4 us -> none  [gather_in_order(): blocks = lax.all_gather(blocks, axes[k], axis=0, tiled=True)]
    all_to_all x0 -> x1, waiting for transfers between devices: none -> 8.97 us  [gather_in_order(): field_out = lax.all_to_all(item_now, x_part, 0, 0)]
    all_to_all x1, starting transfers between devices: 5.39 us -> 13.2 us  [sent_to_all(): lax.all_to_all(jnp.broadcast_to(shard[None], (peers, *shard.shape)), axis...]
    transpose x2 -> x0, local copies, waits for them, and re-layouts: 6.51 us -> none  [gather_in_order(): blocks.transpose(*turned, *range(len(sequence), blocks.ndim))]
  transfers between devices with their start and end apart: 8 -> 5, of which waited for: 5 -> 4; matrix products, arithmetic and copies ran while one was open for 32% -> 28% of each run, Pallas kernels for 0% -> 0%
where the time goes in v1:
time: 481 us; the launch traced here: 479 us
  blocking collectives  205 us (43%)
  matrix products  93 us (19%)
  waiting for transfers between devices  83.4 us (17%)
  other arithmetic  33.5 us (7%)
  starting transfers between devices  31 us (6%)
  local copies, waits for them, and re-layouts  18.2 us (4%)
  between operations  13.7 us (3%)
    all_to_all x9, blocking collectives, gather_in_order(): field_out = lax.all_to_all(item_now, x_part, 0, 0)  194 us
    dot_general x32, matrix products, weighted_values(): jnp.einsum('hqk,khd->qhd', weights, values, preferred_element_type=jnp.fl...  46.6 us
    dot_general x32, matrix products, head_logs(): jnp.einsum('qhd,khd->hqk', queries, keys_block, preferred_element_type=jn...  40.1 us
    all_to_all x1, waiting for transfers between devices, sent_to_all(): lax.all_to_all(jnp.broadcast_to(shard[None], (peers, *shard.shape)), axis...  38.1 us
    all_gather x1, waiting for transfers between devices, gather_axes(): filled = lax.all_gather(filled, axes[number], axis=dim, tiled=True)  26.9 us
    all_to_all x1, starting transfers between devices, summed_on_arrival(): lax.all_to_all(cut_along(shard, dim, peers), axis, 0, 0, tiled=True)  14.1 us
    all_to_all x1, starting transfers between devices, sent_to_all(): lax.all_to_all(jnp.broadcast_to(shard[None], (peers, *shard.shape)), axis...  13.2 us
    another operation x32, other arithmetic, weighted_values(): within = lax.cumsum(grouped, axis=3, reverse=True) - grouped  12.2 us
  transfers between devices with their start and end apart: 5, of which 4 were waited for; matrix products, arithmetic and copies ran while one was open for 28% of the time, Pallas kernels for 0%

profile of v1, /device:TPU:1, one launch (start us, length us, event | category | flops | bytes accessed | tf_op | source)
XLA Modules:
  0.0 479.2 jit_solution(1384306162756783904)
XLA Ops:
  7.3 26.9 %all_to_all.60 = bf16[16,1,128,2]{2,3,1,0:T(2,128)(2,1)S(1)} all-to-all(bf16[16,1,128,2]{2,3,1,0:T(2,128)(2,1)S(1)} %stack.34), channel_id=1, replica_groups=mesh['sp_0'=16,'sp_1'=4,'tp'=8] {'sp_0'}, dimensions={0} | all-to-all | bytes 16384 | tf_op jit(solution)/shard_map/all_to_all | solution.py:28
  34.2 8.3 %all_to_all.61 = bf16[4,16,128,2]{2,1,3,0:T(8,128)(2,1)S(1)} all-to-all(bf16[4,16,128,2]{2,1,3,0:T(8,128)(2,1)S(1)} %stack.35), channel_id=1, replica_groups=mesh['sp_0'=16,'sp_1'=4,'tp'=8] {'sp_1'}, dimensions={0} | all-to-all | bytes 65536 | tf_op jit(solution)/shard_map/all_to_all | solution.py:28
  43.2 15.3 %all_to_all.62 = bf16[16,1,128,64]{2,3,1,0:T(8,128)(2,1)S(1)} all-to-all(bf16[16,1,128,64]{2,3,1,0:T(8,128)(2,1)S(1)} %stack.30), channel_id=1, replica_groups=mesh['sp_0'=16,'sp_1'=4,'tp'=8] {'sp_0'}, dimensions={0} | all-to-all | bytes 524288 | tf_op jit(solution)/shard_map/all_to_all | solution.py:28
  59.3 21.8 %all_to_all.63 = bf16[16,1,128,64]{2,3,1,0:T(8,128)(2,1)S(1)} all-to-all(bf16[16,1,128,64]{2,3,1,0:T(8,128)(2,1)S(1)} %stack.32), channel_id=1, replica_groups=mesh['sp_0'=16,'sp_1'=4,'tp'=8] {'sp_0'}, dimensions={0} | all-to-all | bytes 524288 | tf_op jit(solution)/shard_map/all_to_all | solution.py:28
  81.4 12.9 %all_to_all.64 = bf16[4,16,128,64]{2,3,1,0:T(8,128)(2,1)} all-to-all(bf16[4,16,128,64]{2,3,1,0:T(8,128)(2,1)S(1)} %stack.31), channel_id=1, replica_groups=mesh['sp_0'=16,'sp_1'=4,'tp'=8] {'sp_1'}, dimensions={0} | all-to-all | bytes 2097152 | tf_op jit(solution)/shard_map/all_to_all | solution.py:28
  94.5 12.9 %all_to_all.65 = bf16[4,16,128,64]{2,3,1,0:T(8,128)(2,1)} all-to-all(bf16[4,16,128,64]{2,3,1,0:T(8,128)(2,1)S(1)} %stack.33), channel_id=1, replica_groups=mesh['sp_0'=16,'sp_1'=4,'tp'=8] {'sp_1'}, dimensions={0} | all-to-all | bytes 2097152 | tf_op jit(solution)/shard_map/all_to_all | solution.py:28
  107.5 39.2 %all_to_all.66 = bf16[16,1,128,128]{3,2,1,0:T(8,128)(2,1)S(1)} all-to-all(bf16[16,1,128,128]{3,2,1,0:T(8,128)(2,1)S(1)} %stack.36), channel_id=1, replica_groups=mesh['sp_0'=16,'sp_1'=4,'tp'=8] {'sp_0'}, dimensions={0} | all-to-all | bytes 1048576 | tf_op jit(solution)/shard_map/all_to_all | solution.py:28
  146.8 33.9 %all_to_all.67 = bf16[16,1,128,128]{3,2,1,0:T(8,128)(2,1)S(1)} all-to-all(bf16[16,1,128,128]{3,2,1,0:T(8,128)(2,1)S(1)} %stack.38), channel_id=1, replica_groups=mesh['sp_0'=16,'sp_1'=4,'tp'=8] {'sp_0'}, dimensions={0} | all-to-all | bytes 1048576 | tf_op jit(solution)/shard_map/all_to_all | solution.py:28
  181.2 23.0 %all_to_all.68 = bf16[4,16,128,128]{3,2,1,0:T(8,128)(2,1)} all-to-all(bf16[4,16,128,128]{3,2,1,0:T(8,128)(2,1)S(1)} %stack.37), channel_id=1, replica_groups=mesh['sp_0'=16,'sp_1'=4,'tp'=8] {'sp_1'}, dimensions={0} | all-to-all | bytes 4194304 | tf_op jit(solution)/shard_map/all_to_all | solution.py:28
  206.2 3.7 all-to-all-start.9
  210.8 2.8 copy.37
  213.6 2.7 copy.38
  216.4 3.2 copy.33
  219.6 9.0 %all-to-all-done.9 = bf16[4,16,128,128]{3,2,1,0:T(8,128)(2,1)S(1)} async-done(((bf16[4,16,128,128]{3,2,1,0:T(8,128)(2,1)}), bf16[4,16,128,128]{3,2,1,0:T(8,128)(2,1)S(1)}, u32[]{:S(2)}, u32[]{:S(2)}) %all-to-all-start.9) | async-done | bytes 2097184 | tf_op jit(solution)/shard_map/all_to_all | solution.py:28
  230.0 116.7 %while.20 = (s32[]{:T(128)}, f32[128,1,64]{0,2,1:T(8,128)S(1)}, f32[128,1,128]{0,2,1:T(8,128)S(1)}, f32[1,128]{1,0:T(1,128)S(1)}, f32[1,128]{1,0:T(1,128)S(1)}, ...) while((s32[]{:T(128)}, f32[128,1,64]{0,2,1:T(8,128)S(1)}, ...), condition=%wide.region_9.10_spmd.clone, body=%wide.region_0.9_spmd.clone.sunk | while | flops 57983880 | bytes 5200671 | solution.py:192
  347.4 2.5 broadcast_in_dim.49
  349.9 13.2 %all-to-all-start.10 = ((bf16[8,128,2048]{2,1,0:T(8,128)(2,1)}), bf16[8,128,2048]{2,1,0:T(8,128)(2,1)}, u32[]{:S(2)}, u32[]{:S(2)}) async-start(bf16[8,128,2048]{2,1,0:T(8,128)(2,1)} %broadcast_in_dim.49), calls=%async_computation.10 | async-start | bytes 8388608 | tf_op jit(solution)/shard_map/all_to_all | solution.py:42
  363.1 10.7 %all_gather.10 = bf16[384,128]{0,1:T(8,128)(2,1)} all-gather(bf16[384,32]{0,1:T(8,128)(2,1)S(1)} %copy-done.8), channel_id=1, replica_groups=mesh['sp_0'=16,'sp_1'=4,'tp'=8] {'sp_1'}, dimensions={1}, use_global_device_ids=true | all-gather | bytes 122880 | tf_op jit(solution)/shard_map/all_gather | solution.py:61
  373.8 38.1 %all-to-all-done.10 = bf16[8,128,2048]{2,1,0:T(8,128)(2,1)} async-done(((bf16[8,128,2048]{2,1,0:T(8,128)(2,1)}), bf16[8,128,2048]{2,1,0:T(8,128)(2,1)}, u32[]{:S(2)}, u32[]{:S(2)}) %all-to-all-start.10) | async-done | bytes 4194336 | tf_op jit(solution)/shard_map/all_to_all | solution.py:42
  411.9 3.0 convert_reduce_fusion
  417.6 26.9 %all-gather.5.cloned.1.call-done = bf16[384,2048]{0,1:T(8,128)(2,1)} async-done(((bf16[384,128]{0,1:T(8,128)(2,1)}), bf16[384,2048]{0,1:T(8,128)(2,1)}) %all-gather.5.cloned.1.call-update) | async-done | bytes 1572880 | tf_op jit(solution)/shard_map/all_gather | solution.py:61
  444.5 3.7 convolution_convert_fusion
  448.2 14.1 %all-to-all-start.11 = ((bf16[8,16,2048]{2,1,0:T(8,128)(2,1)}), bf16[8,16,2048]{2,1,0:T(8,128)(2,1)S(1)}, u32[]{:S(2)}, u32[]{:S(2)}) async-start(bf16[8,16,2048]{2,1,0:T(8,128)(2,1)} %bitcast.18), calls=%async_computation.11 | async-start | bytes 1048576 | tf_op jit(solution)/shard_map/all_to_all | solution.py:73
  462.2 9.3 %all-to-all-done.11 = bf16[8,16,2048]{2,1,0:T(8,128)(2,1)S(1)} async-done(((bf16[8,16,2048]{2,1,0:T(8,128)(2,1)}), bf16[8,16,2048]{2,1,0:T(8,128)(2,1)S(1)}, u32[]{:S(2)}, u32[]{:S(2)}) %all-to-all-start.11) | async-done | bytes 524320 | tf_op jit(solution)/shard_map/all_to_all | solution.py:73
  (311 shorter events, 126.8 us)
Async XLA Ops:
  6.5 340.5 %copy-start = (bf16[128,2048]{1,0:T(8,128)(2,1)S(1)}, bf16[128,2048]{1,0:T(8,128)(2,1)}, u32[]{:S(2)}) copy-start(bf16[128,2048]{1,0:T(8,128)(2,1)} %param.25) | copy-start | bytes 1572868
  94.3 13.1 %copy-start.4 = (bf16[128,128]{1,0:T(8,128)(2,1)S(1)}, bf16[128,128]{1,0:T(8,128)(2,1)}, u32[]{:S(2)}) copy-start(bf16[128,128]{1,0:T(8,128)(2,1)} %param.22) | copy-start | bytes 98308
  94.5 52.2 %copy-start.5 = (bf16[128,128]{1,0:T(8,128)(2,1)S(1)}, bf16[128,128]{1,0:T(8,128)(2,1)}, u32[]{:S(2)}) copy-start(bf16[128,128]{1,0:T(8,128)(2,1)} %param.20) | copy-start | bytes 98308
  206.2 3.8 copy-start.6
  206.2 3.8 copy-start.7
  206.2 22.3 %all-to-all-start.9 = ((bf16[4,16,128,128]{3,2,1,0:T(8,128)(2,1)}), bf16[4,16,128,128]{3,2,1,0:T(8,128)(2,1)S(1)}, u32[]{:S(2)}, u32[]{:S(2)}) async-start(bf16[4,16,128,128]{3,2,1,0:T(8,128)(2,1)} %stack.39), calls=%async_computation.9 | async-start | bytes 4194304 | tf_op jit(solution)/shard_map/all_to_all | solution.py:28
  209.9 205.3 %all-gather.3.cloned.1.call-start = ((), (), s32[]{:S(2)}) async-start(), calls=%async_computation.12 | async-start | bytes 3194880 | tf_op jit(solution)/shard_map/all_gather | solution.py:54
  219.5 10.5 %copy-start.2 = (bf16[128,64]{0,1:T(8,128)(2,1)S(1)}, bf16[128,64]{0,1:T(8,128)(2,1)}, u32[]{:S(2)}) copy-start(bf16[128,64]{0,1:T(8,128)(2,1)} %param.17) | copy-start | bytes 49156
  219.6 10.5 %copy-start.9 = (bf16[128,128]{1,0:T(8,128)(2,1)S(1)}, bf16[128,128]{1,0:T(8,128)(2,1)}, u32[]{:S(2)}) copy-start(bf16[128,128]{1,0:T(8,128)(2,1)} %param.18) | copy-start | bytes 98308
  230.0 116.7 %copy-start.3 = (bf16[64,2048]{1,0:T(8,128)(2,1)S(1)}, bf16[64,2048]{1,0:T(8,128)(2,1)}, u32[]{:S(2)}) copy-start(bf16[64,2048]{1,0:T(8,128)(2,1)} %param.24) | copy-start | bytes 786436
  349.9 13.2 %copy-start.8 = (bf16[384,32]{0,1:T(8,128)(2,1)S(1)}, bf16[384,32]{0,1:T(8,128)(2,1)}, u32[]{:S(2)}) copy-start(bf16[384,32]{0,1:T(8,128)(2,1)} %param.29) | copy-start | bytes 73732
  349.9 62.0 %all-to-all-start.10 = ((bf16[8,128,2048]{2,1,0:T(8,128)(2,1)}), bf16[8,128,2048]{2,1,0:T(8,128)(2,1)}, u32[]{:S(2)}, u32[]{:S(2)}) async-start(bf16[8,128,2048]{2,1,0:T(8,128)(2,1)} %broadcast_in_dim.49), calls=%async_computation.10 | async-start | bytes 8388608 | tf_op jit(solution)/shard_map/all_to_all | solution.py:42
  363.1 81.4 %all-gather.5.cloned.1.call-start = ((), (), s32[]{:S(2)}) async-start(), calls=%async_computation.13 | async-start | bytes 1671168 | tf_op jit(solution)/shard_map/all_gather | solution.py:61
  373.8 41.1 %copy-start.1 = (bf16[128,2048]{1,0:T(8,128)(2,1)S(1)}, bf16[128,2048]{1,0:T(8,128)(2,1)}, u32[]{:S(2)}) copy-start(bf16[128,2048]{1,0:T(8,128)(2,1)} %param.16) | copy-start | bytes 1572868
  415.0 0.7 copy-start.10
  448.2 23.4 %all-to-all-start.11 = ((bf16[8,16,2048]{2,1,0:T(8,128)(2,1)}), bf16[8,16,2048]{2,1,0:T(8,128)(2,1)S(1)}, u32[]{:S(2)}, u32[]{:S(2)}) async-start(bf16[8,16,2048]{2,1,0:T(8,128)(2,1)} %bitcast.18), calls=%async_computation.11 | async-start | bytes 1048576 | tf_op jit(solution)/shard_map/all_to_all | solution.py:73
Sparse Core Ops, SparseCore 0:
  213.7 143.9 all-gather.2
  373.9 70.4 all-gather.4
